TPU v7x, 32 devices: a whole 2x2x4 slice. The times are simulated.
32 devices in a mesh: fs: 8 (over z, y), tp: 4 (over x, core).
Axes of the slice: x: 2, y: 2, z: 4, core: 2. Of those that a mesh axis runs over, the one named last changes fastest.
Arguments:
- layer_input: bfloat16 [16384, 2048], P('fs'), may hold values from -6 to 6
- input_cotangent: bfloat16 [16384, 2048], P('fs', 'tp'), may hold values from -6 to 6
- gate_cotangent: bfloat16 [16384, 2048], P('fs', 'tp'), may hold values from -6 to 6
- input_weight: float32 [2048, 2048], P('fs', 'tp'), may hold values from -0.125 to 0.125
- gate_weight: float32 [2048, 2048], P('fs', 'tp'), may hold values from -0.125 to 0.125
- input_basis: bfloat16 [2048, 256], P('fs'), may hold values from -1.81196113 to 1.81196113
- gate_basis: bfloat16 [2048, 256], P('fs'), may hold values from -1.81196113 to 1.81196113
- input_first: float32 [256, 2048], P('fs', 'tp'), may hold values from -10496 to 10496
- input_second: float32 [256, 2048], P('fs', 'tp'), may hold values from 16384 to 491520
- gate_first: float32 [256, 2048], P('fs', 'tp'), may hold values from -10496 to 10496
- gate_second: float32 [256, 2048], P('fs', 'tp'), may hold values from 16384 to 491520
Outputs:
- input_new: float32 [2048, 2048], P('fs', 'tp')
- gate_new: float32 [2048, 2048], P('fs', 'tp')
- input_step: float32 [2048, 2048], P('fs', 'tp')
- gate_step: float32 [2048, 2048], P('fs', 'tp')
- input_first_new: float32 [256, 2048], P('fs', 'tp')
- input_second_new: float32 [256, 2048], P('fs', 'tp')
- gate_first_new: float32 [256, 2048], P('fs', 'tp')
- gate_second_new: float32 [256, 2048], P('fs', 'tp')
- input_copy: bfloat16 [2048, 2048], P(None, 'tp')
- gate_copy: bfloat16 [2048, 2048], P(None, 'tp')
All inputs are finite; a program needn't handle non-finite values.
Results may differ from a plain program's by a relative error of at most 0.0055.
Values may be sent and summed in bfloat16 or wider, within the bound.
A program may use at most 64 MiB of HBM per device.

v0:
```python
import jax
import jax.numpy as jnp
from jax import lax
from jax.sharding import PartitionSpec as P

D = 2048
W = 2048
first_decay = 0.8
second_decay = 0.95
learn_rate = 0.01


def moments(small, first, second):
    first_new = first_decay * first + (1.0 - first_decay) * small
    second_new = second_decay * second + (1.0 - second_decay) * small * small
    direction = (first_new / (jnp.sqrt(second_new) + 1e-08)).astype(jnp.bfloat16)
    return (first_new, second_new, direction)


def split_product(projected, cotangent):
    upper = projected.astype(jnp.bfloat16)
    lower = (projected - upper.astype(jnp.float32)).astype(jnp.bfloat16)
    dims = (((0,), (0,)), ((), ()))
    return lax.dot_general(
        upper, cotangent, dims, preferred_element_type=jnp.float32
    ) + lax.dot_general(lower, cotangent, dims, preferred_element_type=jnp.float32)


def shards(
    layer_input,
    input_cotangent,
    gate_cotangent,
    input_weight,
    gate_weight,
    input_basis,
    gate_basis,
    input_first,
    input_second,
    gate_first,
    gate_second,
):
    pieces = (
        lax.all_gather(input_basis, "fs", axis=0, tiled=True),
        lax.all_gather(gate_basis, "fs", axis=0, tiled=True),
    )
    input_proj = jnp.dot(layer_input, pieces[0], preferred_element_type=jnp.float32)
    gate_proj = jnp.dot(layer_input, pieces[1], preferred_element_type=jnp.float32)
    input_small = split_product(input_proj, input_cotangent)
    gate_small = split_product(gate_proj, gate_cotangent)
    input_part, gate_part = (
        lax.psum_scatter(input_small, "fs", scatter_dimension=0, tiled=True),
        lax.psum_scatter(gate_small, "fs", scatter_dimension=0, tiled=True),
    )
    in_first, in_second, in_direction = moments(input_part, input_first, input_second)
    gt_first, gt_second, gt_direction = moments(gate_part, gate_first, gate_second)
    pieces = (
        lax.all_gather(in_direction, "fs", axis=0, tiled=True),
        lax.all_gather(gt_direction, "fs", axis=0, tiled=True),
    )
    input_update = jnp.dot(input_basis, pieces[0], preferred_element_type=jnp.float32)
    gate_update = jnp.dot(gate_basis, pieces[1], preferred_element_type=jnp.float32)
    input_squares, gate_squares = lax.psum(
        (jnp.sum(input_update * input_update), jnp.sum(gate_update * gate_update)), ("fs", "tp")
    )
    input_factor = jnp.minimum(1.0, 1.0 / jnp.sqrt(input_squares / (D * W) + 1e-06))
    gate_factor = jnp.minimum(1.0, 1.0 / jnp.sqrt(gate_squares / (D * W) + 1e-06))
    input_step = input_factor * input_update
    gate_step = gate_factor * gate_update
    input_new = input_weight - learn_rate * input_step
    gate_new = gate_weight - learn_rate * gate_step
    input_copy, gate_copy = (
        lax.all_gather(input_new.astype(jnp.bfloat16), "fs", axis=0, tiled=True),
        lax.all_gather(gate_new.astype(jnp.bfloat16), "fs", axis=0, tiled=True),
    )
    return (
        input_new,
        gate_new,
        input_step,
        gate_step,
        in_first,
        in_second,
        gt_first,
        gt_second,
        input_copy,
        gate_copy,
    )


def solution(mesh):
    placed = (
        P("fs", None),
        P("fs", "tp"),
        P("fs", "tp"),
        P("fs", "tp"),
        P("fs", "tp"),
        P("fs", None),
        P("fs", None),
        P("fs", "tp"),
        P("fs", "tp"),
        P("fs", "tp"),
        P("fs", "tp"),
    )
    return jax.shard_map(
        shards,
        mesh=mesh,
        in_specs=placed,
        out_specs=(
            P("fs", "tp"),
            P("fs", "tp"),
            P("fs", "tp"),
            P("fs", "tp"),
            P("fs", "tp"),
            P("fs", "tp"),
            P("fs", "tp"),
            P("fs", "tp"),
            P(None, "tp"),
            P(None, "tp"),
        ),
        check_vma=False,
    )
```

profile of v0, /device:TPU:0, one launch (start us, length us, event | category | flops | bytes accessed | tf_op | source)
XLA Modules:
  0.0 412.4 jit_solution(7743012523781812951)
XLA Ops:
  8.7 44.4 %all-gather.7.cloned.1.call-done = bf16[2048,256]{1,0:T(8,128)(2,1)} async-done(((bf16[256,256]{1,0:T(8,128)(2,1)}), bf16[2048,256]{1,0:T(8,128)(2,1)}) %all-gather.7.cloned.1.call-update) | async-done | bytes 1048592 | tf_op jit(solution)/shard_map/all_gather | solution.py:44
  53.2 6.1 %fusion.13 = f32[2048,256]{1,0:T(8,128)S(1)} fusion(bf16[2048,2048]{1,0:T(8,128)(2,1)} %param.11, bf16[2048,256]{1,0:T(8,128)(2,1)} %all-gather.7.cloned.1.call-done), kind=kOutput, calls=%fused_computation.27 | convolution fusion | flops 2147483648 | bytes 11534336 | tf_op jit(solution)/shard_map/dot_general | solution.py:47
  60.0 1.6 convolution_add_fusion
  61.7 32.6 %all-gather.5.cloned.1.call-done = bf16[2048,256]{1,0:T(8,128)(2,1)} async-done(((bf16[256,256]{1,0:T(8,128)(2,1)}), bf16[2048,256]{1,0:T(8,128)(2,1)}) %all-gather.5.cloned.1.call-update) | async-done | bytes 1048592 | tf_op jit(solution)/shard_map/all_gather | solution.py:43
  94.3 6.2 %fusion.12 = f32[2048,256]{1,0:T(8,128)S(1)} fusion(bf16[2048,2048]{1,0:T(8,128)(2,1)} %param.11, bf16[2048,256]{1,0:T(8,128)(2,1)} %all-gather.5.cloned.1.call-done), kind=kOutput, calls=%fused_computation.26 | convolution fusion | flops 2147483648 | bytes 11534336 | tf_op jit(solution)/shard_map/dot_general | solution.py:46
  101.4 1.5 convolution_add_fusion.1
  103.0 1.0 copy.21
  104.0 55.7 %reduce-scatter.5.cloned.1.call-done = f32[32,512]{1,0:T(8,128)} async-done(((f32[256,512]{1,0:T(8,128)}), f32[32,512]{1,0:T(8,128)}) %reduce-scatter.5.cloned.1.call-update) | async-done | bytes 65552 | tf_op jit(solution)/shard_map/reduce_scatter | solution.py:52
  159.7 1.5 divide_convert_fusion
  161.3 30.9 %all_gather.21 = bf16[256,512]{1,0:T(8,128)(2,1)S(1)} all-gather(bf16[32,512]{1,0:T(8,128)(2,1)S(1)} %get-tuple-element.28), channel_id=1, replica_groups=mesh['fs'=8,'tp'=4] {'fs'}, dimensions={0}, use_global_device_ids=true | all-gather | bytes 294912 | tf_op jit(solution)/shard_map/all_gather | solution.py:58
  193.1 32.0 %reduce-scatter.3.cloned.1.call-done = f32[32,512]{1,0:T(8,128)} async-done(((f32[256,512]{1,0:T(8,128)}), f32[32,512]{1,0:T(8,128)}) %reduce-scatter.3.cloned.1.call-update) | async-done | bytes 65552 | tf_op jit(solution)/shard_map/reduce_scatter | solution.py:51
  225.2 1.5 divide_convert_fusion.1
  226.7 30.8 %all_gather.19 = bf16[256,512]{1,0:T(8,128)(2,1)S(1)} all-gather(bf16[32,512]{1,0:T(8,128)(2,1)S(1)} %get-tuple-element.31), channel_id=1, replica_groups=mesh['fs'=8,'tp'=4] {'fs'}, dimensions={0}, use_global_device_ids=true | all-gather | bytes 294912 | tf_op jit(solution)/shard_map/all_gather | solution.py:57
  257.5 1.7 multiply_reduce_fusion.1
  259.2 37.8 %all-reduce = (f32[]{:T(128)}, f32[]{:T(128)}) all-reduce(f32[]{:T(128)} %get-tuple-element.34, f32[]{:T(128)} %get-tuple-element.36), channel_id=1, replica_groups=mesh['fs'=8,'tp'=4] {'fs','tp'}, use_global_device_ids=true, to_apply=%region_2.0 | all-reduce | flops 2 | bytes 16 | tf_op jit(solution)/shard_map/psum | solution.py:62
  297.7 2.2 fusion.9
  299.9 2.0 copy.22
  302.6 2.2 fusion.8
  304.9 2.1 copy.24
  307.0 2.1 copy.26
  311.0 40.2 %all-gather.9.cloned.1.call-done = bf16[2048,512]{0,1:T(8,128)(2,1)} async-done(((bf16[256,512]{0,1:T(8,128)(2,1)}), bf16[2048,512]{0,1:T(8,128)(2,1)}) %all-gather.9.cloned.1.call-update) | async-done | bytes 2097168 | tf_op jit(solution)/shard_map/all_gather | solution.py:72
  351.2 3.9 copy.27
  355.1 46.5 %all-gather.11.cloned.1.call-done = bf16[2048,512]{0,1:T(8,128)(2,1)} async-done(((bf16[256,512]{0,1:T(8,128)(2,1)}), bf16[2048,512]{0,1:T(8,128)(2,1)}) %all-gather.11.cloned.1.call-update) | async-done | bytes 2097168 | tf_op jit(solution)/shard_map/all_gather | solution.py:73
  401.7 3.9 copy.28
  (37 shorter events, 6.2 us)
Async XLA Ops:
  7.2 52.1 %copy-start = (bf16[2048,512]{1,0:T(8,128)(2,1)S(1)}, bf16[2048,512]{1,0:T(8,128)(2,1)}, u32[]{:S(2)}) copy-start(bf16[2048,512]{1,0:T(8,128)(2,1)} %param.13) | copy-start | bytes 6291460
  7.2 46.0 %all-gather.7.cloned.1.call-start = ((), (), s32[]{:S(2)}) async-start(), calls=%async_computation.4 | async-start | bytes 1179648 | tf_op jit(solution)/shard_map/all_gather | solution.py:44
  7.9 86.4 %all-gather.5.cloned.1.call-start = ((), (), s32[]{:S(2)}) async-start(), calls=%async_computation.2 | async-start | bytes 1179648 | tf_op jit(solution)/shard_map/all_gather | solution.py:43
  8.7 151.1 %reduce-scatter.5.cloned.1.call-start = ((), (), s32[]{:S(2)}) async-start(), calls=%async_computation.5 | async-start | bytes 589824 | tf_op jit(solution)/shard_map/reduce_scatter | solution.py:52
  61.6 163.5 %reduce-scatter.3.cloned.1.call-start = ((), (), s32[]{:S(2)}) async-start(), calls=%async_computation.3 | async-start | bytes 589824 | tf_op jit(solution)/shard_map/reduce_scatter | solution.py:51
  94.3 6.2 %copy-start.1 = (bf16[2048,512]{1,0:T(8,128)(2,1)S(1)}, bf16[2048,512]{1,0:T(8,128)(2,1)}, u32[]{:S(2)}) copy-start(bf16[2048,512]{1,0:T(8,128)(2,1)} %param.12) | copy-start | bytes 6291460
  101.3 1.7 copy-start.5
  101.3 58.4 %copy-start.6 = (f32[32,512]{1,0:T(8,128)S(1)}, f32[32,512]{1,0:T(8,128)}, u32[]{:S(2)}) copy-start(f32[32,512]{1,0:T(8,128)} %param.21) | copy-start | bytes 196612
  101.4 58.4 %copy-start.7 = (f32[32,512]{1,0:T(8,128)S(1)}, f32[32,512]{1,0:T(8,128)}, u32[]{:S(2)}) copy-start(f32[32,512]{1,0:T(8,128)} %param.20) | copy-start | bytes 196612
  102.9 89.3 %copy-start.3 = (bf16[256,256]{1,0:T(8,128)(2,1)S(1)}, bf16[256,256]{1,0:T(8,128)(2,1)}, u32[]{:S(2)}) copy-start(bf16[256,256]{1,0:T(8,128)(2,1)} %param.17) | copy-start | bytes 393220
  102.9 122.3 %copy-start.8 = (f32[32,512]{1,0:T(8,128)S(1)}, f32[32,512]{1,0:T(8,128)}, u32[]{:S(2)}) copy-start(f32[32,512]{1,0:T(8,128)} %param.19) | copy-start | bytes 196612
  102.9 122.3 %copy-start.9 = (f32[32,512]{1,0:T(8,128)S(1)}, f32[32,512]{1,0:T(8,128)}, u32[]{:S(2)}) copy-start(f32[32,512]{1,0:T(8,128)} %param.18) | copy-start | bytes 196612
  102.9 154.6 %copy-start.4 = (bf16[256,256]{1,0:T(8,128)(2,1)S(1)}, bf16[256,256]{1,0:T(8,128)(2,1)}, u32[]{:S(2)}) copy-start(bf16[256,256]{1,0:T(8,128)(2,1)} %param.16) | copy-start | bytes 393220
  102.9 248.3 %all-gather.9.cloned.1.call-start = ((), (), s32[]{:S(2)}) async-start(), calls=%async_computation.6 | async-start | bytes 2359296 | tf_op jit(solution)/shard_map/all_gather | solution.py:72
  299.9 101.8 %all-gather.11.cloned.1.call-start = ((), (), s32[]{:S(2)}) async-start(), calls=%async_computation.7 | async-start | bytes 2359296 | tf_op jit(solution)/shard_map/all_gather | solution.py:73
  304.9 4.2 %copy-start.2 = (f32[256,512]{0,1:T(8,128)S(1)}, f32[256,512]{0,1:T(8,128)}, u32[]{:S(2)}) copy-start(f32[256,512]{0,1:T(8,128)} %get-tuple-element.26) | copy-start | bytes 1572868
Sparse Core Ops, SparseCore 0:
  10.1 42.9 all-gather.6
  55.3 39.0 all-gather.4
  98.3 61.4 reduce-scatter.4
  163.5 61.6 reduce-scatter.2
  300.0 51.1 all-gather.8
  353.1 48.5 all-gather.10
where the time goes:
time: 413 us; the launch traced here: 412 us
  waiting for transfers between devices  253 us (61%)
  blocking collectives  99.5 us (24%)
  matrix products  19.5 us (5%)
  local copies, waits for them, and re-layouts  17.1 us (4%)
  between operations  15.6 us (4%)
  other arithmetic  7.44 us (2%)
    reduce_scatter x1, waiting for transfers between devices, shards(): lax.psum_scatter(gate_small, 'fs', scatter_dimension=0, tiled=True)  55.7 us
    all_gather x1, waiting for transfers between devices, shards(): lax.all_gather(gate_new.astype(jnp.bfloat16), 'fs', axis=0, tiled=True)  46.5 us
    all_gather x1, waiting for transfers between devices, shards(): lax.all_gather(gate_basis, 'fs', axis=0, tiled=True)  44.4 us
    all_gather x1, waiting for transfers between devices, shards(): lax.all_gather(input_new.astype(jnp.bfloat16), 'fs', axis=0, tiled=True)  40.2 us
    psum x1, blocking collectives, shards(): lax.psum((jnp.sum(input_update * input_update), jnp.sum(gate_update * gat...  37.8 us
    all_gather x1, waiting for transfers between devices, shards(): lax.all_gather(input_basis, 'fs', axis=0, tiled=True)  32.6 us
    reduce_scatter x1, waiting for transfers between devices, shards(): lax.psum_scatter(input_small, 'fs', scatter_dimension=0, tiled=True)  32 us
    all_gather x1, blocking collectives, shards(): lax.all_gather(gt_direction, 'fs', axis=0, tiled=True)  30.9 us
  transfers between devices with their start and end apart: 6, of which 6 were waited for; matrix products, arithmetic and copies ran while one was open for 8% of the time, Pallas kernels for 0%

commit v1 on v0

--- a/solution.py
+++ b/solution.py
@@ -60,7 +60,8 @@
     input_update = jnp.dot(input_basis, pieces[0], preferred_element_type=jnp.float32)
     gate_update = jnp.dot(gate_basis, pieces[1], preferred_element_type=jnp.float32)
     input_squares, gate_squares = lax.psum(
-        (jnp.sum(input_update * input_update), jnp.sum(gate_update * gate_update)), ("fs", "tp")
+        lax.psum((jnp.sum(input_update * input_update), jnp.sum(gate_update * gate_update)), "tp"),
+        "fs",
     )
     input_factor = jnp.minimum(1.0, 1.0 / jnp.sqrt(input_squares / (D * W) + 1e-06))
     gate_factor = jnp.minimum(1.0, 1.0 / jnp.sqrt(gate_squares / (D * W) + 1e-06))

time: 413 us -> 398 us (0.964)
  blocking collectives: 99.5 us -> 88.1 us
    psum x1, blocking collectives: 37.8 us -> 6.27 us  [shards(): lax.psum((jnp.sum(input_update * input_update), jnp.sum(gate_update * gat...]
    psum x0 -> x1, blocking collectives: none -> 20 us  [shards(): lax.psum(lax.psum((jnp.sum(input_update * input_update), jnp.sum(gate_upd...]
    unnamed x28 -> x26, local copies, waits for them, and re-layouts: 17.1 us -> 16.2 us
  transfers between devices with their start and end apart: 6 -> 6, of which waited for: 6 -> 6; matrix products, arithmetic and copies ran while one was open for 8% -> 9% of each run, Pallas kernels for 0% -> 0%
where the time goes in v1:
time: 398 us; the launch traced here: 397 us
  waiting for transfers between devices  250 us (63%)
  blocking collectives  88.1 us (22%)
  matrix products  19.5 us (5%)
  local copies, waits for them, and re-layouts  16.2 us (4%)
  between operations  15.6 us (4%)
  other arithmetic  7.55 us (2%)
    reduce_scatter x1, waiting for transfers between devices, shards(): lax.psum_scatter(gate_small, 'fs', scatter_dimension=0, tiled=True)  56.5 us
    all_gather x1, waiting for transfers between devices, shards(): lax.all_gather(gate_new.astype(jnp.bfloat16), 'fs', axis=0, tiled=True)  46.5 us
    all_gather x1, waiting for transfers between devices, shards(): lax.all_gather(gate_basis, 'fs', axis=0, tiled=True)  44.4 us
    all_gather x1, waiting for transfers between devices, shards(): lax.all_gather(input_new.astype(jnp.bfloat16), 'fs', axis=0, tiled=True)  36.4 us
    all_gather x1, waiting for transfers between devices, shards(): lax.all_gather(input_basis, 'fs', axis=0, tiled=True)  32.6 us
    reduce_scatter x1, waiting for transfers between devices, shards(): lax.psum_scatter(input_small, 'fs', scatter_dimension=0, tiled=True)  32 us
    all_gather x1, blocking collectives, shards(): lax.all_gather(gt_direction, 'fs', axis=0, tiled=True)  31 us
    all_gather x1, blocking collectives, shards(): lax.all_gather(in_direction, 'fs', axis=0, tiled=True)  30.9 us
  transfers between devices with their start and end apart: 6, of which 6 were waited for; matrix products, arithmetic and copies ran while one was open for 9% of the time, Pallas kernels for 0%

profile of v1, /device:TPU:0, one launch (start us, length us, event | category | flops | bytes accessed | tf_op | source)
XLA Modules:
  0.0 397.4 jit_solution(8143283661222558773)
XLA Ops:
  8.7 44.4 %all-gather.7.cloned.1.call-done = bf16[2048,256]{1,0:T(8,128)(2,1)} async-done(((bf16[256,256]{1,0:T(8,128)(2,1)}), bf16[2048,256]{1,0:T(8,128)(2,1)}) %all-gather.7.cloned.1.call-update) | async-done | bytes 1048592 | tf_op jit(solution)/shard_map/all_gather | solution.py:44
  53.2 6.1 %fusion.13 = f32[2048,256]{1,0:T(8,128)S(1)} fusion(bf16[2048,2048]{1,0:T(8,128)(2,1)} %param.11, bf16[2048,256]{1,0:T(8,128)(2,1)} %all-gather.7.cloned.1.call-done), kind=kOutput, calls=%fused_computation.27 | convolution fusion | flops 2147483648 | bytes 11534336 | tf_op jit(solution)/shard_map/dot_general | solution.py:47
  60.0 1.6 convolution_add_fusion
  61.7 32.6 %all-gather.5.cloned.1.call-done = bf16[2048,256]{1,0:T(8,128)(2,1)} async-done(((bf16[256,256]{1,0:T(8,128)(2,1)}), bf16[2048,256]{1,0:T(8,128)(2,1)}) %all-gather.5.cloned.1.call-update) | async-done | bytes 1048592 | tf_op jit(solution)/shard_map/all_gather | solution.py:43
  94.3 6.2 %fusion.12 = f32[2048,256]{1,0:T(8,128)S(1)} fusion(bf16[2048,2048]{1,0:T(8,128)(2,1)} %param.11, bf16[2048,256]{1,0:T(8,128)(2,1)} %all-gather.5.cloned.1.call-done), kind=kOutput, calls=%fused_computation.26 | convolution fusion | flops 2147483648 | bytes 11534336 | tf_op jit(solution)/shard_map/dot_general | solution.py:46
  101.4 1.5 convolution_add_fusion.1
  103.2 56.5 %reduce-scatter.5.cloned.1.call-done = f32[32,512]{1,0:T(8,128)} async-done(((f32[256,512]{1,0:T(8,128)}), f32[32,512]{1,0:T(8,128)}) %reduce-scatter.5.cloned.1.call-update) | async-done | bytes 65552 | tf_op jit(solution)/shard_map/reduce_scatter | solution.py:52
  159.7 1.5 divide_convert_fusion
  161.3 31.0 %all_gather.21 = bf16[256,512]{1,0:T(8,128)(2,1)S(1)} all-gather(bf16[32,512]{1,0:T(8,128)(2,1)S(1)} %get-tuple-element.30), channel_id=1, replica_groups=mesh['fs'=8,'tp'=4] {'fs'}, dimensions={0}, use_global_device_ids=true | all-gather | bytes 294912 | tf_op jit(solution)/shard_map/all_gather | solution.py:58
  193.2 32.0 %reduce-scatter.3.cloned.1.call-done = f32[32,512]{1,0:T(8,128)} async-done(((f32[256,512]{1,0:T(8,128)}), f32[32,512]{1,0:T(8,128)}) %reduce-scatter.3.cloned.1.call-update) | async-done | bytes 65552 | tf_op jit(solution)/shard_map/reduce_scatter | solution.py:51
  225.2 1.6 divide_convert_fusion.1
  226.8 30.9 %all_gather.19 = bf16[256,512]{1,0:T(8,128)(2,1)S(1)} all-gather(bf16[32,512]{1,0:T(8,128)(2,1)S(1)} %get-tuple-element.33), channel_id=1, replica_groups=mesh['fs'=8,'tp'=4] {'fs'}, dimensions={0}, use_global_device_ids=true | all-gather | bytes 294912 | tf_op jit(solution)/shard_map/all_gather | solution.py:57
  257.7 1.7 multiply_reduce_fusion.1
  259.3 6.3 %all-reduce.1 = (f32[]{:T(128)}, f32[]{:T(128)}) all-reduce(f32[]{:T(128)} %get-tuple-element.36, f32[]{:T(128)} %get-tuple-element.38), channel_id=1, replica_groups=mesh['fs'=8,'tp'=4] {'tp'}, use_global_device_ids=true, to_apply=%region_2.0 | all-reduce | flops 2 | bytes 16 | tf_op jit(solution)/shard_map/psum | solution.py:63
  265.6 20.0 %all-reduce = (f32[]{:T(128)}, f32[]{:T(128)}) all-reduce(f32[]{:T(128)} %get-tuple-element.22, f32[]{:T(128)} %get-tuple-element.23), channel_id=1, replica_groups=mesh['fs'=8,'tp'=4] {'fs'}, use_global_device_ids=true, to_apply=%region_3.0 | all-reduce | flops 2 | bytes 16 | tf_op jit(solution)/shard_map/psum | solution.py:62
  286.3 2.2 fusion.9
  288.5 2.0 copy.22
  291.3 2.3 fusion.8
  293.6 2.1 copy.24
  295.7 2.0 copy.26
  299.7 36.4 %all-gather.9.cloned.1.call-done = bf16[2048,512]{0,1:T(8,128)(2,1)} async-done(((bf16[256,512]{0,1:T(8,128)(2,1)}), bf16[2048,512]{0,1:T(8,128)(2,1)}) %all-gather.9.cloned.1.call-update) | async-done | bytes 2097168 | tf_op jit(solution)/shard_map/all_gather | solution.py:73
  336.1 3.9 copy.27
  340.1 46.5 %all-gather.11.cloned.1.call-done = bf16[2048,512]{0,1:T(8,128)(2,1)} async-done(((bf16[256,512]{0,1:T(8,128)(2,1)}), bf16[2048,512]{0,1:T(8,128)(2,1)}) %all-gather.11.cloned.1.call-update) | async-done | bytes 2097168 | tf_op jit(solution)/shard_map/all_gather | solution.py:74
  386.6 3.9 copy.28
  (36 shorter events, 6.3 us)
Async XLA Ops:
  7.2 52.1 %copy-start = (bf16[2048,512]{1,0:T(8,128)(2,1)S(1)}, bf16[2048,512]{1,0:T(8,128)(2,1)}, u32[]{:S(2)}) copy-start(bf16[2048,512]{1,0:T(8,128)(2,1)} %param.13) | copy-start | bytes 6291460
  7.2 46.0 %all-gather.7.cloned.1.call-start = ((), (), s32[]{:S(2)}) async-start(), calls=%async_computation.4 | async-start | bytes 1179648 | tf_op jit(solution)/shard_map/all_gather | solution.py:44
  7.9 86.4 %all-gather.5.cloned.1.call-start = ((), (), s32[]{:S(2)}) async-start(), calls=%async_computation.2 | async-start | bytes 1179648 | tf_op jit(solution)/shard_map/all_gather | solution.py:43
  8.7 151.1 %reduce-scatter.5.cloned.1.call-start = ((), (), s32[]{:S(2)}) async-start(), calls=%async_computation.5 | async-start | bytes 589824 | tf_op jit(solution)/shard_map/reduce_scatter | solution.py:52
  61.6 163.6 %reduce-scatter.3.cloned.1.call-start = ((), (), s32[]{:S(2)}) async-start(), calls=%async_computation.3 | async-start | bytes 589824 | tf_op jit(solution)/shard_map/reduce_scatter | solution.py:51
  94.3 6.2 %copy-start.1 = (bf16[2048,512]{1,0:T(8,128)(2,1)S(1)}, bf16[2048,512]{1,0:T(8,128)(2,1)}, u32[]{:S(2)}) copy-start(bf16[2048,512]{1,0:T(8,128)(2,1)} %param.12) | copy-start | bytes 6291460
  101.3 1.6 copy-start.6
  101.3 58.4 %copy-start.7 = (f32[32,512]{1,0:T(8,128)S(1)}, f32[32,512]{1,0:T(8,128)}, u32[]{:S(2)}) copy-start(f32[32,512]{1,0:T(8,128)} %param.21) | copy-start | bytes 196612
  101.4 58.4 %copy-start.8 = (f32[32,512]{1,0:T(8,128)S(1)}, f32[32,512]{1,0:T(8,128)}, u32[]{:S(2)}) copy-start(f32[32,512]{1,0:T(8,128)} %param.20) | copy-start | bytes 196612
  102.9 89.4 %copy-start.4 = (bf16[256,256]{1,0:T(8,128)(2,1)S(1)}, bf16[256,256]{1,0:T(8,128)(2,1)}, u32[]{:S(2)}) copy-start(bf16[256,256]{1,0:T(8,128)(2,1)} %param.17) | copy-start | bytes 393220
  102.9 154.8 %copy-start.5 = (bf16[256,256]{1,0:T(8,128)(2,1)S(1)}, bf16[256,256]{1,0:T(8,128)(2,1)}, u32[]{:S(2)}) copy-start(bf16[256,256]{1,0:T(8,128)(2,1)} %param.16) | copy-start | bytes 393220
  102.9 233.2 %all-gather.9.cloned.1.call-start = ((), (), s32[]{:S(2)}) async-start(), calls=%async_computation.6 | async-start | bytes 2359296 | tf_op jit(solution)/shard_map/all_gather | solution.py:73
  288.5 98.1 %all-gather.11.cloned.1.call-start = ((), (), s32[]{:S(2)}) async-start(), calls=%async_computation.7 | async-start | bytes 2359296 | tf_op jit(solution)/shard_map/all_gather | solution.py:74
  291.3 6.4 %copy-start.3 = (f32[256,512]{0,1:T(8,128)S(1)}, f32[256,512]{0,1:T(8,128)}, u32[]{:S(2)}) copy-start(f32[256,512]{0,1:T(8,128)} %get-tuple-element.28) | copy-start | bytes 1572868
  293.5 5.2 %copy-start.2 = (f32[256,512]{0,1:T(8,128)S(1)}, f32[256,512]{0,1:T(8,128)}, u32[]{:S(2)}) copy-start(f32[256,512]{0,1:T(8,128)} %get-tuple-element.29) | copy-start | bytes 1572868
Sparse Core Ops, SparseCore 0:
  10.1 42.9 all-gather.6
  55.3 39.0 all-gather.4
  98.3 61.4 reduce-scatter.4
  163.5 61.6 reduce-scatter.2
  288.6 47.4 all-gather.8
  338.0 48.5 all-gather.10
